TPU v7x, 32 devices: a whole 2x2x4 slice. The times are simulated.
32 devices in a mesh: rep: 2 (over y), fs: 4 (over z), tp: 4 (over x, core).
Axes of the slice: x: 2, y: 2, z: 4, core: 2. Of those that a mesh axis runs over, the one named last changes fastest.
Arguments:
- tokens: bfloat16 [4096, 2048], P(('rep', 'fs'), 'tp'), may hold values from -6 to 6
- outer_gate: float32 [2048, 512], P('fs', 'tp'), may hold values from -0.125 to 0.125
- inner_gate: float32 [2048, 512], P('fs', 'tp'), may hold values from -0.125 to 0.125
- mixer_value: float32 [2048, 512], P('fs', 'tp'), may hold values from -0.125 to 0.125
- mixer_scales: float32 [3, 512], P(None, 'tp'), may hold values from 0.5 to 2
- mixer_taps: float32 [3, 512], P(None, 'tp'), may hold values from -3.5 to 3.5
- mixer_out: float32 [512, 2048], P('fs', 'tp'), may hold values from -0.25 to 0.25
- out_scale: float32 [2048], P('tp'), may hold values from 0.3 to 3
- first_gain: float32 [2048], replicated, may hold values from 0.1 to 1.9
- first_shift: float32 [2048], replicated, may hold values from -2 to 2
- up_proj: float32 [2048, 3072], P('fs', 'tp'), may hold values from -0.125 to 0.125
- gate_proj: float32 [2048, 3072], P('fs', 'tp'), may hold values from -0.125 to 0.125
- up_scales: float32 [2, 3072], P(None, 'tp'), may hold values from 0.5 to 2
- ffn_taps: float32 [3, 2, 3072], P(None, None, 'tp'), may hold values from -3.5 to 3.5
- ffn_shift: float32 [2, 3072], P(None, 'tp'), may hold values from -3 to 3
- down_proj: float32 [3072, 2048], P('fs', 'tp'), may hold values from -0.109375 to 0.109375
- down_scale: float32 [2048], P('tp'), may hold values from 0.3 to 3
- second_gain: float32 [2048], replicated, may hold values from 0.1 to 1.9
- second_shift: float32 [2048], replicated, may hold values from -2 to 2
Outputs:
- layer_out: bfloat16 [4096, 2048], P(('rep', 'fs'), 'tp')
All inputs are finite; a program needn't handle non-finite values.
Results may differ from a plain program's by a relative error of at most 0.017.
Values may be sent and summed in bfloat16 or wider, within the bound.
A program may use at most 64 MiB of HBM per device.

v0:
```python
import jax
import jax.numpy as jnp
from jax import lax
from jax.sharding import PartitionSpec as P

LEN = 128
norm_eps = 1e-05
residual_weight = 8.0**0.25


def causal_mix(signal, kernel_taps):
    sequences = signal.reshape(-1, LEN, signal.shape[-1])
    padded = jnp.pad(sequences, ((0, 0), (2, 0), (0, 0)))
    mixed = (
        kernel_taps[0] * padded[:, :-2]
        + kernel_taps[1] * padded[:, 1:-1]
        + kernel_taps[2] * padded[:, 2:]
    )
    return mixed.reshape(signal.shape)


def lowered(matrix):
    return matrix.astype(jnp.bfloat16)


def single_fold(operand, portion):
    return jnp.dot(operand, portion, preferred_element_type=jnp.float32)


def fold_step(operand, pieces):
    result = []
    for number in range(len(pieces)):
        result.append(jnp.dot(operand, pieces[number], preferred_element_type=jnp.float32))
    return tuple(result)


def own_columns(vector, own_width):
    return lax.dynamic_slice_in_dim(vector, lax.axis_index("tp") * own_width, own_width, 0)


def scaled_norm(summed, average, spread, gain_vector, shift_vector):
    return (summed - average) * lax.rsqrt(spread + norm_eps) * gain_vector + shift_vector


def local(
    tokens,
    outer_gate,
    inner_gate,
    mixer_value,
    mixer_scales,
    mixer_taps,
    mixer_out,
    out_scale,
    first_gain,
    first_shift,
    up_proj,
    gate_proj,
    up_scales,
    ffn_taps,
    ffn_shift,
    down_proj,
    down_scale,
    second_gain,
    second_shift,
):
    own_width = tokens.shape[1]
    full_width = own_width * lax.axis_size("tp")
    token_whole = lax.all_gather(tokens, "tp", axis=1, tiled=True)
    outer_part, inner_part, value_part = fold_step(
        token_whole,
        (
            lax.all_gather(lowered(outer_gate), "fs", axis=0, tiled=True),
            lax.all_gather(lowered(inner_gate), "fs", axis=0, tiled=True),
            lax.all_gather(lowered(mixer_value), "fs", axis=0, tiled=True),
        ),
    )
    outer_part = (outer_part * mixer_scales[0]).astype(jnp.bfloat16)
    inner_part = (inner_part * mixer_scales[1]).astype(jnp.bfloat16)
    value_part = (value_part * mixer_scales[2]).astype(jnp.bfloat16)
    product = inner_part.astype(jnp.float32) * value_part.astype(jnp.float32)
    mixed_conv = (outer_part.astype(jnp.float32) * causal_mix(product, mixer_taps)).astype(
        jnp.bfloat16
    )
    conv_whole = lax.all_gather(mixed_conv, "tp", axis=1, tiled=True)
    mixer_sum = (
        single_fold(conv_whole, lax.all_gather(lowered(mixer_out), "fs", axis=0, tiled=True))
        * out_scale
    )
    first_sum = residual_weight * tokens.astype(jnp.float32) + mixer_sum
    row_total, row_square = lax.psum(
        (jnp.sum(first_sum, 1, keepdims=True), jnp.sum(first_sum * first_sum, 1, keepdims=True)),
        "tp",
    )
    average = row_total / full_width
    spread = row_square / full_width - average * average
    normed = scaled_norm(
        first_sum,
        average,
        spread,
        own_columns(first_gain, own_width),
        own_columns(first_shift, own_width),
    ).astype(jnp.bfloat16)
    normed_whole = lax.all_gather(normed, "tp", axis=1, tiled=True)
    up_matrix, gate_matrix = (
        lax.all_gather(lowered(up_proj), "fs", axis=0, tiled=True),
        lax.all_gather(lowered(gate_proj), "fs", axis=0, tiled=True),
    )
    up_linear = jnp.dot(normed_whole, up_matrix, preferred_element_type=jnp.float32)
    gate_linear = jnp.dot(normed_whole, gate_matrix, preferred_element_type=jnp.float32)
    up_linear = up_linear * up_scales[0]
    gate_linear = gate_linear * up_scales[1]
    up_mixed = causal_mix(up_linear, ffn_taps[:, 0]) + ffn_shift[0]
    gate_mixed = causal_mix(gate_linear, ffn_taps[:, 1]) + ffn_shift[1]
    hidden = (up_mixed * jax.nn.silu(gate_mixed)).astype(jnp.bfloat16)
    hidden_whole = lax.all_gather(hidden, "tp", axis=1, tiled=True)
    ffn_sum = (
        single_fold(hidden_whole, lax.all_gather(lowered(down_proj), "fs", axis=0, tiled=True))
        * down_scale
    )
    second_sum = residual_weight * normed.astype(jnp.float32) + ffn_sum
    second_total, second_square = lax.psum(
        (jnp.sum(second_sum, 1, keepdims=True), jnp.sum(second_sum * second_sum, 1, keepdims=True)),
        "tp",
    )
    second_average = second_total / full_width
    second_spread = second_square / full_width - second_average * second_average
    return scaled_norm(
        second_sum,
        second_average,
        second_spread,
        own_columns(second_gain, own_width),
        own_columns(second_shift, own_width),
    ).astype(jnp.bfloat16)


def solution(mesh):
    return jax.shard_map(
        local,
        mesh=mesh,
        in_specs=(
            P(("rep", "fs"), "tp"),
            P("fs", "tp"),
            P("fs", "tp"),
            P("fs", "tp"),
            P(None, "tp"),
            P(None, "tp"),
            P("fs", "tp"),
            P("tp"),
            P(),
            P(),
            P("fs", "tp"),
            P("fs", "tp"),
            P(None, "tp"),
            P(None, None, "tp"),
            P(None, "tp"),
            P("fs", "tp"),
            P("tp"),
            P(),
            P(),
        ),
        out_specs=P(("rep", "fs"), "tp"),
        check_vma=False,
    )
```

profile of v0, /device:TPU:0, one launch (start us, length us, event | category | flops | bytes accessed | tf_op | source)
XLA Modules:
  0.0 314.0 jit_solution(7180715300881190758)
XLA Ops:
  6.5 0.0 all-gather.7.cloned.1.call-start
  6.5 0.7 all-gather.7.cloned.1.call-update
  7.3 0.0 copy-start.2
  7.3 0.0 copy-start.6
  7.3 0.0 all-gather.11.cloned.1.call-start
  7.3 2.4 convert_element_type.76
  9.8 0.0 all-gather.11.cloned.1.call-update
  9.8 0.0 all-gather.9.cloned.1.call-start
  9.9 1.0 copy.22
  11.0 0.0 copy-done.9
  11.0 0.0 copy-start.13
  11.0 0.0 copy-start.14
  11.0 0.8 dynamic_slice.12
  11.8 0.8 dynamic_slice.13
  12.5 17.4 %all_gather.36 = bf16[2048,128]{1,0:T(8,128)(2,1)S(1)} all-gather(bf16[512,128]{1,0:T(8,128)(2,1)S(1)} %convert_element_type.69), channel_id=1, replica_groups=mesh['rep'=2,'fs'=4,'tp'=4] {'fs'}, dimensions={0}, use_global_device_ids=true | all-gather | bytes 655360 | tf_op jit(solution)/shard_map/all_gather | solution.py:74
  29.9 16.9 %all_gather.35 = bf16[2048,128]{1,0:T(8,128)(2,1)S(1)} all-gather(bf16[512,128]{1,0:T(8,128)(2,1)S(1)} %convert_element_type.66), channel_id=1, replica_groups=mesh['rep'=2,'fs'=4,'tp'=4] {'fs'}, dimensions={0}, use_global_device_ids=true | all-gather | bytes 655360 | tf_op jit(solution)/shard_map/all_gather | solution.py:73
  46.8 22.6 %all_gather.34 = bf16[2048,128]{1,0:T(8,128)(2,1)S(1)} all-gather(bf16[512,128]{1,0:T(8,128)(2,1)S(1)} %convert_element_type.63), channel_id=1, replica_groups=mesh['rep'=2,'fs'=4,'tp'=4] {'fs'}, dimensions={0}, use_global_device_ids=true | all-gather | bytes 655360 | tf_op jit(solution)/shard_map/all_gather | solution.py:72
  69.4 20.2 %all_gather.38 = bf16[512,512]{1,0:T(8,128)(2,1)S(1)} all-gather(bf16[128,512]{1,0:T(8,128)(2,1)S(1)} %convert_element_type.73), channel_id=1, replica_groups=mesh['rep'=2,'fs'=4,'tp'=4] {'fs'}, dimensions={0}, use_global_device_ids=true | all-gather | bytes 655360 | tf_op jit(solution)/shard_map/all_gather | solution.py:86
  89.6 0.0 copy-done.13
  89.6 0.0 all-gather.7.cloned.1.call-done
  89.6 2.5 fusion.20
  92.1 0.7 fusion.18
  92.8 0.1 fusion.23
  92.9 0.0 copy-start.5
  92.9 0.0 copy-start.15
  92.9 0.7 fusion.15
  93.7 7.0 %all_gather.37 = bf16[512,512]{1,0:T(8,128)(2,1)S(1)} all-gather(bf16[512,128]{1,0:T(8,128)(2,1)S(1)} %fusion.15), channel_id=1, replica_groups=mesh['rep'=2,'fs'=4,'tp'=4] {'tp'}, dimensions={1}, use_global_device_ids=true | all-gather | bytes 655360 | tf_op jit(solution)/shard_map/all_gather | solution.py:84
  100.7 0.0 copy-done.15
  100.7 0.6 fusion.26
  101.3 0.0 copy-start.3
  101.3 7.0 %all-reduce.4 = (f32[512,1]{0,1:T(1,128)S(1)}, f32[512,1]{0,1:T(1,128)S(1)}) all-reduce(f32[512,1]{0,1:T(1,128)S(1)} %bitcast.57, f32[512,1]{0,1:T(1,128)S(1)} %bitcast.56), channel_id=1, replica_groups=mesh['rep'=2,'fs'=4,'tp'=4] {'tp'}, use_global_device_ids=true, to_apply=%region_3.4 | all-reduce | flops 1024 | bytes 8192 | tf_op jit(solution)/shard_map/psum | solution.py:90
  108.3 1.0 add_convert_fusion.1
  109.3 0.0 all-gather.9.cloned.1.call-update
  109.3 0.0 copy-start.4
  109.3 0.0 all-gather.13.cloned.1.call-start
  109.4 1.0 convert_element_type.77
  110.4 0.0 all-gather.13.cloned.1.call-update
  110.4 0.0 copy-start.11
  110.4 0.0 copy-start.12
  110.4 0.0 copy-start.10
  110.5 0.0 all-gather.17.cloned.1.call-start
  110.5 0.5 copy-done.4
  111.0 1.0 convert_element_type.79
  112.0 0.0 all-gather.17.cloned.1.call-update
  112.0 0.0 all-gather.15.cloned.1.call-start
  112.1 0.1 slice_reduce_fusion.4
  112.2 2.2 all-gather.11.cloned.1.call-done
  114.4 23.7 %all-gather.9.cloned.1.call-done = bf16[512,2048]{0,1:T(8,128)(2,1)} async-done(((bf16[512,512]{0,1:T(8,128)(2,1)}), bf16[512,2048]{0,1:T(8,128)(2,1)}) %all-gather.9.cloned.1.call-update) | async-done | bytes 2097168 | tf_op jit(solution)/shard_map/all_gather | solution.py:103
  138.2 4.4 %convolution_multiply_fusion.1 = f32[512,768]{1,0:T(8,128)S(1)} fusion(bf16[512,2048]{0,1:T(8,128)(2,1)} %all-gather.9.cloned.1.call-done, bf16[2048,768]{1,0:T(8,128)(2,1)} %all-gather.11.cloned.1.call-done, f32[768]{0:T(1024)S(1)} %get-tuple-element.18), kind=kOutput, calls=%fused_computation.17 | convolution fusion | flops 1611005952 | bytes 6818816 | tf_op jit(solution)/shard_map/dot_general | solution.py:108
  142.5 60.5 %all-gather.13.cloned.1.call-done = bf16[2048,768]{1,0:T(8,128)(2,1)} async-done(((bf16[512,768]{1,0:T(8,128)(2,1)}), bf16[2048,768]{1,0:T(8,128)(2,1)}) %all-gather.13.cloned.1.call-update) | async-done | bytes 3145744 | tf_op jit(solution)/shard_map/all_gather | solution.py:106
  203.1 4.4 %convolution_multiply_fusion = f32[512,768]{1,0:T(8,128)S(1)} fusion(bf16[512,2048]{0,1:T(8,128)(2,1)} %all-gather.9.cloned.1.call-done, bf16[2048,768]{1,0:T(8,128)(2,1)} %all-gather.13.cloned.1.call-done, f32[768]{0:T(1024)S(1)} %get-tuple-element.17), kind=kOutput, calls=%fused_computation.16 | convolution fusion | flops 1611005952 | bytes 6818816 | tf_op jit(solution)/shard_map/dot_general | solution.py:109
  207.4 0.9 fusion.2
  208.4 0.0 copy-start.1
  208.4 0.0 copy-start.16
  208.4 1.4 fusion.9
  209.8 0.0 all-gather.15.cloned.1.call-update
  209.8 0.8 dynamic_slice.14
  210.5 0.8 dynamic_slice.15
  211.3 55.3 %all-gather.17.cloned.1.call-done = bf16[3072,512]{1,0:T(8,128)(2,1)} async-done(((bf16[768,512]{1,0:T(8,128)(2,1)}), bf16[3072,512]{1,0:T(8,128)(2,1)}) %all-gather.17.cloned.1.call-update) | async-done | bytes 3145744 | tf_op jit(solution)/shard_map/all_gather | solution.py:117
  266.6 28.6 %all-gather.15.cloned.1.call-done = bf16[512,3072]{1,0:T(8,128)(2,1)} async-done(((bf16[512,768]{1,0:T(8,128)(2,1)}), bf16[512,3072]{1,0:T(8,128)(2,1)}) %all-gather.15.cloned.1.call-update) | async-done | bytes 3145744 | tf_op jit(solution)/shard_map/all_gather | solution.py:115
  295.2 4.8 %fusion.25 = (f32[512]{0:T(512)S(1)}, f32[512]{0:T(512)S(1)}, f32[512,512]{0,1:T(8,128)S(1)}) fusion(f32[512]{0:T(512)S(1)} %copy-done.16, bf16[512,3072]{1,0:T(8,128)(2,1)} %all-gather.15.cloned.1.call-done, bf16[3072,512]{1,0:T(8,128)(2,1)} %all-gather.17.cloned.1.call-done, bf16[512,512]{0,1:T(8,128)(2,1)S(1)} %copy-done.1), kind=kOutput, calls=%fused_computation.64 | convolution fusion | flops 1612446720 | bytes 7870464 | tf_op jit(solution)/shard_map/dot_general | solution.py:27
  300.0 5.9 %all-reduce.3 = (f32[512,1]{0,1:T(1,128)S(1)}, f32[512,1]{0,1:T(1,128)S(1)}) all-reduce(f32[512,1]{0,1:T(1,128)S(1)} %bitcast.59, f32[512,1]{0,1:T(1,128)S(1)} %bitcast.58), channel_id=1, replica_groups=mesh['rep'=2,'fs'=4,'tp'=4] {'tp'}, use_global_device_ids=true, to_apply=%region_7.8 | all-reduce | flops 1024 | bytes 8192 | tf_op jit(solution)/shard_map/psum | solution.py:121
  305.9 0.2 add_convert_fusion
  306.1 1.0 copy.23
  (27 shorter events, 0.2 us)
Async XLA Ops:
  6.5 83.1 %all-gather.7.cloned.1.call-start = ((), (), s32[]{:S(2)}) async-start(), calls=%async_computation | async-start | bytes 2621440 | tf_op jit(solution)/shard_map/all_gather | solution.py:68
  7.3 2.6 copy-start.2
  7.3 3.6 %copy-start.6 = (f32[512,128]{1,0:T(8,128)S(1)}, f32[512,128]{1,0:T(8,128)}, u32[]{:S(2)}) copy-start(f32[512,128]{1,0:T(8,128)} %param.22) | copy-start | bytes 786436
  7.3 107.2 %all-gather.11.cloned.1.call-start = ((), (), s32[]{:S(2)}) async-start(), calls=%async_computation.2 | async-start | bytes 3932160 | tf_op jit(solution)/shard_map/all_gather | solution.py:105
  9.8 1.1 copy-start.7
  9.8 1.2 copy-start.8
  9.8 1.2 copy-start.9
  9.8 128.4 %all-gather.9.cloned.1.call-start = ((), (), s32[]{:S(2)}) async-start(), calls=%async_computation.1 | async-start | bytes 2621440 | tf_op jit(solution)/shard_map/all_gather | solution.py:103
  11.0 78.6 %copy-start.13 = (f32[3,128]{1,0:T(4,128)S(1)}, f32[3,128]{1,0:T(4,128)}, u32[]{:S(2)}) copy-start(f32[3,128]{1,0:T(4,128)} %param.23) | copy-start | bytes 4612
  11.0 78.6 %copy-start.14 = (f32[3,128]{1,0:T(4,128)S(1)}, f32[3,128]{1,0:T(4,128)}, u32[]{:S(2)}) copy-start(f32[3,128]{1,0:T(4,128)} %param.24) | copy-start | bytes 4612
  89.6 2.5 copy-start
  92.9 7.8 %copy-start.5 = (bf16[512,512]{0,1:T(8,128)(2,1)S(1)}, bf16[512,512]{0,1:T(8,128)(2,1)}, u32[]{:S(2)}) copy-start(bf16[512,512]{0,1:T(8,128)(2,1)} %copy.22) | copy-start | bytes 1572868
  92.9 7.8 %copy-start.15 = (f32[512]{0:T(512)S(1)}, f32[512]{0:T(512)}, u32[]{:S(2)}) copy-start(f32[512]{0:T(512)} %param.26) | copy-start | bytes 6148
  101.3 8.1 %copy-start.3 = (f32[512,768]{1,0:T(8,128)S(1)}, f32[512,768]{1,0:T(8,128)}, u32[]{:S(2)}) copy-start(f32[512,768]{1,0:T(8,128)} %param.30) | copy-start | bytes 4718596
  109.3 1.7 copy-start.4
  109.3 93.8 %all-gather.13.cloned.1.call-start = ((), (), s32[]{:S(2)}) async-start(), calls=%async_computation.3 | async-start | bytes 3932160 | tf_op jit(solution)/shard_map/all_gather | solution.py:106
  110.4 1.6 copy-start.11
  110.4 1.7 copy-start.12
  110.4 1.7 copy-start.10
  110.5 156.2 %all-gather.17.cloned.1.call-start = ((), (), s32[]{:S(2)}) async-start(), calls=%async_computation.5 | async-start | bytes 3932160 | tf_op jit(solution)/shard_map/all_gather | solution.py:117
  112.0 183.2 %all-gather.15.cloned.1.call-start = ((), (), s32[]{:S(2)}) async-start(), calls=%async_computation.4 | async-start | bytes 3932160 | tf_op jit(solution)/shard_map/all_gather | solution.py:115
  208.4 86.8 %copy-start.1 = (bf16[512,512]{0,1:T(8,128)(2,1)S(1)}, bf16[512,512]{0,1:T(8,128)(2,1)}, u32[]{:S(2)}) copy-start(bf16[512,512]{0,1:T(8,128)(2,1)} %add_convert_fusion.1) | copy-start | bytes 1572868
  208.4 86.8 %copy-start.16 = (f32[512]{0:T(512)S(1)}, f32[512]{0:T(512)}, u32[]{:S(2)}) copy-start(f32[512]{0:T(512)} %param.35) | copy-start | bytes 6148
Sparse Core Ops, SparseCore 0:
  8.9 25.2 all-gather.6
  35.8 78.6 all-gather.10
  116.0 22.1 all-gather.8
  139.6 63.4 all-gather.12
  204.5 62.0 all-gather.16
  268.0 27.1 all-gather.14
where the time goes:
time: 314 us
  waiting for transfers between devices  171 us (54%)
  blocking collectives  96.9 us (31%)
  matrix products  18 us (6%)
  between operations  13.8 us (4%)
  other arithmetic  8.13 us (3%)
  local copies, waits for them, and re-layouts  5.76 us (2%)
    all_gather x1, waiting for transfers between devices, local(): lax.all_gather(lowered(gate_proj), 'fs', axis=0, tiled=True)  60.5 us
    all_gather x1, waiting for transfers between devices, local(): lax.all_gather(lowered(down_proj), 'fs', axis=0, tiled=True)  55.3 us
    all_gather x1, waiting for transfers between devices, local(): hidden_whole = lax.all_gather(hidden, 'tp', axis=1, tiled=True)  28.6 us
    all_gather x1, waiting for transfers between devices, local(): normed_whole = lax.all_gather(normed, 'tp', axis=1, tiled=True)  23.7 us
    all_gather x1, blocking collectives, local(): lax.all_gather(lowered(outer_gate), 'fs', axis=0, tiled=True)  22.6 us
    all_gather x1, blocking collectives, local(): lax.all_gather(lowered(mixer_out), 'fs', axis=0, tiled=True)  20.2 us
    all_gather x1, blocking collectives, local(): lax.all_gather(lowered(mixer_value), 'fs', axis=0, tiled=True)  17.4 us
    all_gather x1, blocking collectives, local(): lax.all_gather(lowered(inner_gate), 'fs', axis=0, tiled=True)  16.9 us
  transfers between devices with their start and end apart: 6, of which 5 were waited for; matrix products, arithmetic and copies ran while one was open for 8% of the time, Pallas kernels for 0%

commit v1 on v0

--- a/solution.py
+++ b/solution.py
@@ -6,6 +6,22 @@
 LEN = 128
 norm_eps = 1e-05
 residual_weight = 8.0**0.25
+
+
+def step_on_row(block_in, dimension_no):
+    nd = lax.psum(1, axis_name="tp")
+    pieces_in = [(k0, (k0 + 1) % nd) for k0 in range(nd)]
+
+    def save_the_task(small):
+        if len(small) == nd:
+            return small
+        return save_the_task([lax.ppermute(small[0], axis_name="tp", perm=pieces_in), *small])
+
+    return jnp.roll(
+        jnp.concatenate(save_the_task([block_in]), dimension_no),
+        (lax.axis_index("tp") + 1) * block_in.shape[dimension_no],
+        dimension_no,
+    )
 
 
 def causal_mix(signal, kernel_taps):
@@ -112,7 +128,7 @@
     up_mixed = causal_mix(up_linear, ffn_taps[:, 0]) + ffn_shift[0]
     gate_mixed = causal_mix(gate_linear, ffn_taps[:, 1]) + ffn_shift[1]
     hidden = (up_mixed * jax.nn.silu(gate_mixed)).astype(jnp.bfloat16)
-    hidden_whole = lax.all_gather(hidden, "tp", axis=1, tiled=True)
+    hidden_whole = step_on_row(hidden, 1)
     ffn_sum = (
         single_fold(hidden_whole, lax.all_gather(lowered(down_proj), "fs", axis=0, tiled=True))
         * down_scale

time: 314 us -> 286 us (0.911)
  waiting for transfers between devices: 171 us -> 136 us
  local copies, waits for them, and re-layouts: 5.76 us -> 13.7 us
    all_gather x1, waiting for transfers between devices: 55.3 us -> 15.5 us  [local(): lax.all_gather(lowered(down_proj), 'fs', axis=0, tiled=True)]
    ppermute x0 -> x3, waiting for transfers between devices: none -> 32.7 us  [save_the_task(): lax.ppermute(small[0], axis_name='tp', perm=pieces_in)]
    all_gather x1 -> x0, waiting for transfers between devices: 28.6 us -> none  [local(): hidden_whole = lax.all_gather(hidden, 'tp', axis=1, tiled=True)]
    unnamed x35 -> x42, local copies, waits for them, and re-layouts: 1.59 us -> 8.51 us
  transfers between devices with their start and end apart: 6 -> 8, of which waited for: 5 -> 7; matrix products, arithmetic and copies ran while one was open for 8% -> 11% of each run, Pallas kernels for 0% -> 0%
where the time goes in v1:
time: 286 us
  waiting for transfers between devices  136 us (48%)
  blocking collectives  97.3 us (34%)
  matrix products  18.4 us (6%)
  local copies, waits for them, and re-layouts  13.7 us (5%)
  between operations  13.4 us (5%)
  other arithmetic  7.24 us (3%)
    all_gather x1, waiting for transfers between devices, local(): lax.all_gather(lowered(gate_proj), 'fs', axis=0, tiled=True)  60.5 us
    ppermute x3, waiting for transfers between devices, save_the_task(): lax.ppermute(small[0], axis_name='tp', perm=pieces_in)  32.7 us
    all_gather x1, waiting for transfers between devices, local(): normed_whole = lax.all_gather(normed, 'tp', axis=1, tiled=True)  23.7 us
    all_gather x1, blocking collectives, local(): lax.all_gather(lowered(outer_gate), 'fs', axis=0, tiled=True)  22.5 us
    all_gather x1, blocking collectives, local(): lax.all_gather(lowered(mixer_out), 'fs', axis=0, tiled=True)  20.2 us
    all_gather x1, blocking collectives, local(): lax.all_gather(lowered(mixer_value), 'fs', axis=0, tiled=True)  17.4 us
    all_gather x1, blocking collectives, local(): lax.all_gather(lowered(inner_gate), 'fs', axis=0, tiled=True)  16.9 us
    all_gather x1, waiting for transfers between devices, local(): lax.all_gather(lowered(down_proj), 'fs', axis=0, tiled=True)  15.5 us
  transfers between devices with their start and end apart: 8, of which 7 were waited for; matrix products, arithmetic and copies ran while one was open for 11% of the time, Pallas kernels for 0%

profile of v1, /device:TPU:0, one launch (start us, length us, event | category | flops | bytes accessed | tf_op | source)
XLA Modules:
  0.0 285.9 jit_solution(7963090939256901115)
XLA Ops:
  6.5 0.0 all-gather.6.cloned.1.call-start
  6.5 0.7 all-gather.6.cloned.1.call-update
  7.3 0.0 all-gather.10.cloned.1.call-start
  7.3 2.4 convert_element_type.76
  9.8 0.0 all-gather.10.cloned.1.call-update
  9.8 0.0 all-gather.8.cloned.1.call-start
  9.9 0.0 copy-done.2
  9.9 1.0 copy.22
  11.0 0.8 dynamic_slice.16
  11.8 0.8 dynamic_slice.17
  12.5 17.4 %all_gather.33 = bf16[2048,128]{1,0:T(8,128)(2,1)S(1)} all-gather(bf16[512,128]{1,0:T(8,128)(2,1)S(1)} %convert_element_type.69), channel_id=1, replica_groups=mesh['rep'=2,'fs'=4,'tp'=4] {'fs'}, dimensions={0}, use_global_device_ids=true | all-gather | bytes 655360 | tf_op jit(solution)/shard_map/all_gather | solution.py:90
  29.9 16.9 %all_gather.32 = bf16[2048,128]{1,0:T(8,128)(2,1)S(1)} all-gather(bf16[512,128]{1,0:T(8,128)(2,1)S(1)} %convert_element_type.66), channel_id=1, replica_groups=mesh['rep'=2,'fs'=4,'tp'=4] {'fs'}, dimensions={0}, use_global_device_ids=true | all-gather | bytes 655360 | tf_op jit(solution)/shard_map/all_gather | solution.py:89
  46.8 22.5 %all_gather.31 = bf16[2048,128]{1,0:T(8,128)(2,1)S(1)} all-gather(bf16[512,128]{1,0:T(8,128)(2,1)S(1)} %convert_element_type.63), channel_id=1, replica_groups=mesh['rep'=2,'fs'=4,'tp'=4] {'fs'}, dimensions={0}, use_global_device_ids=true | all-gather | bytes 655360 | tf_op jit(solution)/shard_map/all_gather | solution.py:88
  69.3 20.2 %all_gather.35 = bf16[512,512]{1,0:T(8,128)(2,1)S(1)} all-gather(bf16[128,512]{1,0:T(8,128)(2,1)S(1)} %convert_element_type.73), channel_id=1, replica_groups=mesh['rep'=2,'fs'=4,'tp'=4] {'fs'}, dimensions={0}, use_global_device_ids=true | all-gather | bytes 655360 | tf_op jit(solution)/shard_map/all_gather | solution.py:102
  89.6 0.0 all-gather.6.cloned.1.call-done
  89.6 2.5 fusion.27
  92.1 0.7 fusion.25
  92.8 0.0 copy-start.5
  92.8 0.0 copy-start.15
  92.8 0.1 fusion.30
  92.9 0.7 fusion.22
  93.6 7.1 %all_gather.34 = bf16[512,512]{1,0:T(8,128)(2,1)S(1)} all-gather(bf16[512,128]{1,0:T(8,128)(2,1)S(1)} %fusion.22), channel_id=1, replica_groups=mesh['rep'=2,'fs'=4,'tp'=4] {'tp'}, dimensions={1}, use_global_device_ids=true | all-gather | bytes 655360 | tf_op jit(solution)/shard_map/all_gather | solution.py:100
  100.7 0.6 fusion.34
  101.3 6.8 %all-reduce.4 = (f32[512,1]{0,1:T(1,128)S(1)}, f32[512,1]{0,1:T(1,128)S(1)}) all-reduce(f32[512,1]{0,1:T(1,128)S(1)} %bitcast.58, f32[512,1]{0,1:T(1,128)S(1)} %bitcast.57), channel_id=1, replica_groups=mesh['rep'=2,'fs'=4,'tp'=4] {'tp'}, use_global_device_ids=true, to_apply=%region_3.4 | all-reduce | flops 1024 | bytes 8192 | tf_op jit(solution)/shard_map/psum | solution.py:106
  108.2 1.0 add_convert_fusion.1
  109.2 0.0 all-gather.8.cloned.1.call-update
  109.2 0.0 all-gather.12.cloned.1.call-start
  109.2 1.0 convert_element_type.77
  110.3 0.0 all-gather.12.cloned.1.call-update
  110.3 0.0 all-gather.14.cloned.1.call-start
  110.3 0.5 copy-done.4
  110.9 1.0 convert_element_type.79
  111.8 0.0 all-gather.14.cloned.1.call-update
  111.9 0.0 copy-done.10
  111.9 0.1 slice_reduce_fusion.4
  112.0 2.4 all-gather.10.cloned.1.call-done
  114.4 23.7 %all-gather.8.cloned.1.call-done = bf16[512,2048]{0,1:T(8,128)(2,1)} async-done(((bf16[512,512]{0,1:T(8,128)(2,1)}), bf16[512,2048]{0,1:T(8,128)(2,1)}) %all-gather.8.cloned.1.call-update) | async-done | bytes 2097168 | tf_op jit(solution)/shard_map/all_gather | solution.py:119
  138.2 4.4 %convolution_multiply_fusion.1 = f32[512,768]{1,0:T(8,128)S(1)} fusion(bf16[512,2048]{0,1:T(8,128)(2,1)} %all-gather.8.cloned.1.call-done, bf16[2048,768]{1,0:T(8,128)(2,1)} %all-gather.10.cloned.1.call-done, f32[768]{0:T(1024)S(1)} %get-tuple-element.18), kind=kOutput, calls=%fused_computation.19 | convolution fusion | flops 1611005952 | bytes 6818816 | tf_op jit(solution)/shard_map/dot_general | solution.py:124
  142.5 60.5 %all-gather.12.cloned.1.call-done = bf16[2048,768]{1,0:T(8,128)(2,1)} async-done(((bf16[512,768]{1,0:T(8,128)(2,1)}), bf16[2048,768]{1,0:T(8,128)(2,1)}) %all-gather.12.cloned.1.call-update) | async-done | bytes 3145744 | tf_op jit(solution)/shard_map/all_gather | solution.py:122
  203.1 4.4 %convolution_multiply_fusion = f32[512,768]{1,0:T(8,128)S(1)} fusion(bf16[512,2048]{0,1:T(8,128)(2,1)} %all-gather.8.cloned.1.call-done, bf16[2048,768]{1,0:T(8,128)(2,1)} %all-gather.12.cloned.1.call-done, f32[768]{0:T(1024)S(1)} %get-tuple-element.17), kind=kOutput, calls=%fused_computation.18 | convolution fusion | flops 1611005952 | bytes 6818816 | tf_op jit(solution)/shard_map/dot_general | solution.py:125
  207.4 0.9 fusion.4
  208.4 0.5 fusion.11
  208.8 0.1 collective-permute-start
  208.9 11.4 %collective-permute-done = bf16[512,768]{1,0:T(8,128)(2,1)S(1)} collective-permute-done((bf16[512,768]{1,0:T(8,128)(2,1)S(1)}, bf16[512,768]{1,0:T(8,128)(2,1)S(1)}, u32[]{:S(2)}, u32[]{:S(2)}) %collective-permute-start) | collective-permute-done | bytes 786464 | tf_op jit(solution)/shard_map/ppermute | solution.py:18
  220.3 0.0 collective-permute-start.1
  220.3 11.4 %collective-permute-done.1 = bf16[512,768]{1,0:T(8,128)(2,1)S(1)} collective-permute-done((bf16[512,768]{1,0:T(8,128)(2,1)S(1)}, bf16[512,768]{1,0:T(8,128)(2,1)S(1)}, u32[]{:S(2)}, u32[]{:S(2)}) %collective-permute-start.1) | collective-permute-done | bytes 786464 | tf_op jit(solution)/shard_map/ppermute | solution.py:18
  231.7 0.0 collective-permute-start.2
  231.7 0.8 dynamic_slice.19
  232.5 0.8 dynamic_slice.20
  233.2 9.9 %collective-permute-done.2 = bf16[512,768]{1,0:T(8,128)(2,1)S(1)} collective-permute-done((bf16[512,768]{1,0:T(8,128)(2,1)S(1)}, bf16[512,768]{1,0:T(8,128)(2,1)S(1)}, u32[]{:S(2)}, u32[]{:S(2)}) %collective-permute-start.2) | collective-permute-done | bytes 786464 | tf_op jit(solution)/shard_map/ppermute | solution.py:18
  243.1 1.0 constant_dynamic-update-slice_fusion.7
  244.1 1.0 constant_dynamic-update-slice_fusion.6
  245.1 1.0 constant_dynamic-update-slice_fusion.5
  246.1 1.0 constant_dynamic-update-slice_fusion.4
  247.0 1.0 constant_dynamic-update-slice_fusion.3
  248.1 1.0 constant_dynamic-update-slice_fusion.2
  249.1 1.0 constant_dynamic-update-slice_fusion.1
  250.1 1.0 constant_dynamic-update-slice_fusion
  251.1 15.5 %all-gather.14.cloned.1.call-done = bf16[3072,512]{1,0:T(8,128)(2,1)} async-done(((bf16[768,512]{1,0:T(8,128)(2,1)}), bf16[3072,512]{1,0:T(8,128)(2,1)}) %all-gather.14.cloned.1.call-update) | async-done | bytes 3145744 | tf_op jit(solution)/shard_map/all_gather | solution.py:133
  266.6 0.0 copy-done.1
  266.6 5.2 %fusion.33 = (f32[512]{0:T(512)S(1)}, f32[512]{0:T(512)S(1)}, f32[512,512]{0,1:T(8,128)S(1)}) fusion(f32[512]{0:T(512)S(1)} %copy-done.16, bf16[3072,512]{1,0:T(8,128)(2,1)} %all-gather.14.cloned.1.call-done, bf16[512,6144]{1,0:T(8,128)(2,1)} %constant_dynamic-update-slice_fusion, s32[]{:T(128)S(6)} %select_n.21, bf16[512,512]{0,1:T(8,128)(2,1)S(1)} %copy-done.1), kind=kOutput, calls=%fused_computation.75 | convolution fusion | flops 1612446720 | bytes 7870468 | tf_op jit(solution)/shard_map/dot_general | solution.py:43
  271.8 6.4 %all-reduce.3 = (f32[512,1]{0,1:T(1,128)S(1)}, f32[512,1]{0,1:T(1,128)S(1)}) all-reduce(f32[512,1]{0,1:T(1,128)S(1)} %bitcast.56, f32[512,1]{0,1:T(1,128)S(1)} %bitcast.55), channel_id=1, replica_groups=mesh['rep'=2,'fs'=4,'tp'=4] {'tp'}, use_global_device_ids=true, to_apply=%region_7.8 | all-reduce | flops 1024 | bytes 8192 | tf_op jit(solution)/shard_map/psum | solution.py:137
  278.2 0.2 add_convert_fusion
  278.4 1.0 copy.23
  (38 shorter events, 0.2 us)
Async XLA Ops:
  6.5 3.3 %copy-start.2 = (bf16[512,512]{1,0:T(8,128)(2,1)S(1)}, bf16[512,512]{1,0:T(8,128)(2,1)}, u32[]{:S(2)}) copy-start(bf16[512,512]{1,0:T(8,128)(2,1)} %param.19) | copy-start | bytes 1572868
  6.5 83.1 %all-gather.6.cloned.1.call-start = ((), (), s32[]{:S(2)}) async-start(), calls=%async_computation | async-start | bytes 2621440 | tf_op jit(solution)/shard_map/all_gather | solution.py:84
  7.3 3.6 %copy-start.6 = (f32[512,128]{1,0:T(8,128)S(1)}, f32[512,128]{1,0:T(8,128)}, u32[]{:S(2)}) copy-start(f32[512,128]{1,0:T(8,128)} %param.22) | copy-start | bytes 786436
  7.3 3.6 %copy-start.7 = (f32[512,128]{1,0:T(8,128)S(1)}, f32[512,128]{1,0:T(8,128)}, u32[]{:S(2)}) copy-start(f32[512,128]{1,0:T(8,128)} %param.21) | copy-start | bytes 786436
  7.3 3.7 %copy-start.8 = (f32[512,128]{1,0:T(8,128)S(1)}, f32[512,128]{1,0:T(8,128)}, u32[]{:S(2)}) copy-start(f32[512,128]{1,0:T(8,128)} %param.20) | copy-start | bytes 786436
  7.3 107.2 %all-gather.10.cloned.1.call-start = ((), (), s32[]{:S(2)}) async-start(), calls=%async_computation.2 | async-start | bytes 3932160 | tf_op jit(solution)/shard_map/all_gather | solution.py:121
  9.8 1.2 copy-start.9
  9.8 128.3 %all-gather.8.cloned.1.call-start = ((), (), s32[]{:S(2)}) async-start(), calls=%async_computation.1 | async-start | bytes 2621440 | tf_op jit(solution)/shard_map/all_gather | solution.py:119
  10.9 78.7 %copy-start.13 = (f32[3,128]{1,0:T(4,128)S(1)}, f32[3,128]{1,0:T(4,128)}, u32[]{:S(2)}) copy-start(f32[3,128]{1,0:T(4,128)} %param.23) | copy-start | bytes 4612
  10.9 78.7 %copy-start.14 = (f32[3,128]{1,0:T(4,128)S(1)}, f32[3,128]{1,0:T(4,128)}, u32[]{:S(2)}) copy-start(f32[3,128]{1,0:T(4,128)} %param.24) | copy-start | bytes 4612
  89.6 2.5 copy-start
  92.8 7.9 %copy-start.5 = (bf16[512,512]{0,1:T(8,128)(2,1)S(1)}, bf16[512,512]{0,1:T(8,128)(2,1)}, u32[]{:S(2)}) copy-start(bf16[512,512]{0,1:T(8,128)(2,1)} %copy.22) | copy-start | bytes 1572868
  92.8 7.9 %copy-start.15 = (f32[512]{0:T(512)S(1)}, f32[512]{0:T(512)}, u32[]{:S(2)}) copy-start(f32[512]{0:T(512)} %param.26) | copy-start | bytes 6148
  100.7 8.5 %copy-start.3 = (f32[512,768]{1,0:T(8,128)S(1)}, f32[512,768]{1,0:T(8,128)}, u32[]{:S(2)}) copy-start(f32[512,768]{1,0:T(8,128)} %param.30) | copy-start | bytes 4718596
  109.2 1.7 copy-start.4
  109.2 93.9 %all-gather.12.cloned.1.call-start = ((), (), s32[]{:S(2)}) async-start(), calls=%async_computation.3 | async-start | bytes 3932160 | tf_op jit(solution)/shard_map/all_gather | solution.py:122
  110.3 1.6 copy-start.11
  110.3 1.6 copy-start.10
  110.3 1.7 copy-start.12
  110.3 156.3 %all-gather.14.cloned.1.call-start = ((), (), s32[]{:S(2)}) async-start(), calls=%async_computation.4 | async-start | bytes 3932160 | tf_op jit(solution)/shard_map/all_gather | solution.py:133
  208.8 11.5 %collective-permute-start = (bf16[512,768]{1,0:T(8,128)(2,1)S(1)}, bf16[512,768]{1,0:T(8,128)(2,1)S(1)}, u32[]{:S(2)}, u32[]{:S(2)}) collective-permute-start(bf16[512,768]{1,0:T(8,128)(2,1)S(1)} %fusion.11), channel_id=1, source_target_pairs={{0,1},{1,2},{2,3},{3,0},{4,5},{5,6},{6,7},{7,4},{8,9},{9,10},{10,1... | collective-permute-start | bytes 2359304 | tf_op jit(solution)/shard_map/ppermute | solution.py:18
  220.3 11.4 %collective-permute-start.1 = (bf16[512,768]{1,0:T(8,128)(2,1)S(1)}, bf16[512,768]{1,0:T(8,128)(2,1)S(1)}, u32[]{:S(2)}, u32[]{:S(2)}) collective-permute-start(bf16[512,768]{1,0:T(8,128)(2,1)S(1)} %collective-permute-done), channel_id=1, source_target_pairs={{0,1},{1,2},{2,3},{3,0},{4,5},{5,6},{6,7},{7,4},{8,9},{9,10},{10,1... | collective-permute-start | bytes 2359304 | tf_op jit(solution)/shard_map/ppermute | solution.py:18
  231.7 11.4 %collective-permute-start.2 = (bf16[512,768]{1,0:T(8,128)(2,1)S(1)}, bf16[512,768]{1,0:T(8,128)(2,1)S(1)}, u32[]{:S(2)}, u32[]{:S(2)}) collective-permute-start(bf16[512,768]{1,0:T(8,128)(2,1)S(1)} %collective-permute-done.1), channel_id=1, source_target_pairs={{0,1},{1,2},{2,3},{3,0},{4,5},{5,6},{6,7},{7,4},{8,9},{9,10},{10,1... | collective-permute-start | bytes 2359304 | tf_op jit(solution)/shard_map/ppermute | solution.py:18
  248.1 18.5 %copy-start.1 = (bf16[512,512]{0,1:T(8,128)(2,1)S(1)}, bf16[512,512]{0,1:T(8,128)(2,1)}, u32[]{:S(2)}) copy-start(bf16[512,512]{0,1:T(8,128)(2,1)} %add_convert_fusion.1) | copy-start | bytes 1572868
  248.1 18.5 %copy-start.16 = (f32[512]{0:T(512)S(1)}, f32[512]{0:T(512)}, u32[]{:S(2)}) copy-start(f32[512]{0:T(512)} %param.35) | copy-start | bytes 6148
Sparse Core Ops, SparseCore 0:
  8.9 25.2 all-gather.5
  35.8 78.6 all-gather.9
  116.0 22.1 all-gather.7
  139.6 63.4 all-gather.11
  204.5 62.0 all-gather.13
